TPU v7x, 32 devices: a whole 2x2x4 slice. The times are simulated.
32 devices in a mesh: grp: 2 (over y), sp: 4 (over z), tp: 4 (over x, core).
Axes of the slice: x: 2, y: 2, z: 4, core: 2. Of those that a mesh axis runs over, the one named last changes fastest.
Arguments:
- query_latent: bfloat16 [1024, 768], P(('grp', 'sp')), parts along dimension 0, may hold values from -6 to 6
- key_latent: bfloat16 [1024, 256], P(('grp', 'sp', 'tp')), parts along dimension 0, may hold values from -20 to 20
- rotary_key: bfloat16 [1024, 64], P(('grp', 'sp', 'tp')), parts along dimension 0, may hold values from -1000 to 1000
- query_gain: float32 [768], replicated, may hold values from 0.1 to 1.9
- latent_gain: float32 [256], replicated, may hold values from 0.1 to 1.9
- query_up: bfloat16 [768, 3072], P(None, 'tp'), may hold values from -0.21875 to 0.21875
- key_up: bfloat16 [256, 2048], P(None, 'tp'), may hold values from -0.375 to 0.375
- value_up: bfloat16 [256, 2048], P(None, 'tp'), may hold values from -0.375 to 0.375
- out_gain: float32 [2048], P('tp'), may hold values from 0.1 to 1.9
- out_weight: bfloat16 [2048, 4096], P('sp', 'tp'), may hold values from -0.125 to 0.125
Outputs:
- mixed: bfloat16 [1024, 4096], P(('grp', 'sp'), 'tp'), parts along dimension 0
There are 2 independent parts, one for each index of `grp`. A program takes and returns all parts, laid end to end along the dimension named above; an argument that names none is the same for every part. Nothing has to cross between parts.
All inputs are finite; a program needn't handle non-finite values.
Results may differ from a plain program's by a relative error of at most 0.02.
The roundings to bfloat16 on the way count: a program that leaves them out, or rounds other values in their place, can miss the bound.
Values may be sent and summed in bfloat16 or wider, within the bound.
A program may use at most 128 MiB of HBM per device.

v0:
```python
import jax
import jax.numpy as jnp
from jax import lax
from jax.sharding import PartitionSpec as P

HEADS = 16
NOPE_DIM = 128
ROPE_DIM = 64
VALUE_DIM = 128
KVRANK = 256
norm_eps = 1e-06
rope_theta = 10000.0


def rms_scaled(inputs, gain_vec):
    widened = inputs.astype(jnp.float32)
    return (
        widened
        * lax.rsqrt(jnp.mean(widened * widened, axis=-1, keepdims=True) + norm_eps)
        * gain_vec
    )


def rotate_half(inputs, positions):
    half_width = inputs.shape[-1] // 2
    inverse = rope_theta ** (-jnp.arange(half_width, dtype=jnp.float32) / half_width)
    angles = positions[:, None] * inverse[None, :]
    if inputs.ndim == 3:
        angles = angles[:, None, :]
    cosine = jnp.cos(angles)
    sine = jnp.sin(angles)
    widened = inputs.astype(jnp.float32)
    first = widened[..., :half_width]
    second = widened[..., half_width:]
    return jnp.concatenate(
        [first * cosine - second * sine, second * cosine + first * sine], axis=-1
    )


def on_device(
    query_latent,
    key_latent,
    rotary_key,
    query_gain,
    latent_gain,
    query_up,
    key_up,
    value_up,
    out_gain,
    out_weight,
):
    block_rows = query_latent.shape[0]
    row_count = key_latent.shape[0]
    head_local = key_up.shape[1] // NOPE_DIM
    block_start = lax.axis_index("sp") * block_rows
    own_start = block_start + lax.axis_index("tp") * row_count
    score_scale = (NOPE_DIM + ROPE_DIM) ** (-0.5)
    normed = rms_scaled(query_latent, query_gain).astype(jnp.bfloat16)
    query_full = jnp.dot(normed, query_up, preferred_element_type=jnp.float32).astype(jnp.bfloat16)
    query_full = query_full.reshape(block_rows, head_local, NOPE_DIM + ROPE_DIM)
    query_positions = (block_start + jnp.arange(block_rows, dtype=jnp.int32)).astype(jnp.float32)
    query_plain = query_full[..., :NOPE_DIM]
    query_turned = rotate_half(query_full[..., NOPE_DIM:], query_positions).astype(jnp.bfloat16)
    latent_normed = rms_scaled(key_latent, latent_gain).astype(jnp.bfloat16)
    own_positions = (own_start + jnp.arange(row_count, dtype=jnp.int32)).astype(jnp.float32)
    key_turned = rotate_half(rotary_key, own_positions).astype(jnp.bfloat16)
    running_max = jnp.full((block_rows, head_local), -1e30, jnp.float32)
    running_sum = jnp.zeros((block_rows, head_local), jnp.float32)
    weighted = jnp.zeros((block_rows, head_local, KVRANK), jnp.float32)
    latents = lax.all_gather(latent_normed, ("sp", "tp"), axis=0, tiled=True)
    turned_keys = lax.all_gather(key_turned, ("sp", "tp"), axis=0, tiled=True)
    portion_rows = latents.shape[0]
    step_rows = min(portion_rows, 2048)
    for begin in range(0, portion_rows, step_rows):
        latent_part = latents[begin : begin + step_rows]
        turned_part = turned_keys[begin : begin + step_rows]
        key_plain = jnp.dot(latent_part, key_up, preferred_element_type=jnp.float32).astype(
            jnp.bfloat16
        )
        key_plain = key_plain.reshape(latent_part.shape[0], head_local, NOPE_DIM)
        scores = jnp.einsum(
            "qhd,khd->qhk", query_plain, key_plain, preferred_element_type=jnp.float32
        )
        scores = scores + jnp.einsum(
            "qhd,kd->qhk", query_turned, turned_part, preferred_element_type=jnp.float32
        )
        scores = scores * score_scale
        new_max = jnp.maximum(running_max, jnp.max(scores, axis=-1))
        rescale = jnp.exp(running_max - new_max)
        expo = jnp.exp(scores - new_max[..., None])
        running_sum = running_sum * rescale + jnp.sum(expo, axis=-1)
        weighted = weighted * rescale[..., None] + jnp.einsum(
            "qhk,kc->qhc",
            expo.astype(jnp.bfloat16),
            latent_part,
            preferred_element_type=jnp.float32,
        )
        running_max = new_max
    final_state = (running_max, running_sum, weighted)
    running_max, running_sum, weighted = final_state
    latent_mix = (weighted / running_sum[..., None]).astype(jnp.bfloat16)
    value_heads = value_up.reshape(KVRANK, head_local, VALUE_DIM)
    head_out = jnp.einsum(
        "qhc,chd->qhd", latent_mix, value_heads, preferred_element_type=jnp.float32
    ).astype(jnp.bfloat16)
    head_out = head_out.reshape(block_rows, head_local * VALUE_DIM)
    widened = head_out.astype(jnp.float32)
    square_part = jnp.sum(widened * widened, axis=1)
    gained = (widened * out_gain).astype(jnp.bfloat16)
    all_gained, square_parts = (
        lax.all_gather(gained, "tp", axis=1, tiled=True),
        lax.all_gather(square_part[:, None].astype(jnp.bfloat16), "tp", axis=1, tiled=True).astype(
            jnp.float32
        ),
    )
    all_squares = jnp.sum(square_parts, axis=1)
    own_sums = jnp.dot(
        all_gained,
        lax.all_gather(out_weight, "sp", axis=0, tiled=True),
        preferred_element_type=jnp.float32,
    )
    mean_square = all_squares / (HEADS * VALUE_DIM)
    return (own_sums * lax.rsqrt(mean_square + norm_eps)[:, None]).astype(jnp.bfloat16)


def solution(mesh):
    in_specs = (
        P(("grp", "sp"), None),
        P(("grp", "sp", "tp"), None),
        P(("grp", "sp", "tp"), None),
        P(),
        P(),
        P(None, "tp"),
        P(None, "tp"),
        P(None, "tp"),
        P("tp"),
        P("sp", "tp"),
    )
    out_specs = P(("grp", "sp"), "tp")
    return jax.shard_map(
        on_device, mesh=mesh, in_specs=in_specs, out_specs=out_specs, check_vma=False
    )
```

profile of v0, /device:TPU:0, one launch (start us, length us, event | category | flops | bytes accessed | tf_op | source)
XLA Modules:
  0.0 103.9 jit_solution(13197024730950181628)
XLA Ops:
  6.5 0.0 copy-start
  6.5 0.0 copy-start.1
  6.5 0.0 all-gather.3.cloned.1.call-start
  6.5 0.7 all-gather.3.cloned.1.call-update
  7.3 1.0 %fusion.13 = f32[128]{0:T(128)S(1)} fusion(bf16[128,768]{1,0:T(8,128)(2,1)} %param.10), kind=kLoop, calls=%fused_computation.19 | loop fusion | flops 294784 | bytes 197120 | tf_op jit(solution)/shard_map/reduce_sum | solution.py:19
  8.3 0.0 copy-done
  8.3 1.3 %convolution_convert_fusion.1 = bf16[128,768]{1,0:T(8,128)(2,1)S(1)} fusion(bf16[768,768]{1,0:T(8,128)(2,1)S(1)} %copy-done, bf16[128,768]{1,0:T(8,128)(2,1)} %param.10, f32[768]{0:T(1024)} %param.13, f32[128]{0:T(128)S(1)} %add_rsqrt_fusion.1), kind=kOutput, calls=%fused_computation.9 | convolution fusion | flops 151486464 | bytes 1576448 | tf_op jit(solution)/shard_map/dot_general | solution.py:59
  9.6 0.2 copy.21
  9.8 0.7 convert_element_type.94
  10.5 1.1 %copy.30 = bf16[256,512]{0,1:T(8,128)(2,1)S(1)} copy(bf16[256,512]{1,0:T(8,128)(2,1)} %param.17) | data formatting | bytes 524288 | tf_op jit(solution)/shard_map/reshape | solution.py:102
  11.6 0.1 fusion.37
  11.8 0.1 pad_maximum_fusion
  11.8 24.3 %all_gather.16 = bf16[512,64]{1,0:T(8,128)(2,1)S(1)} all-gather(bf16[32,64]{1,0:T(8,128)(2,1)S(1)} %pad_maximum_fusion), channel_id=1, replica_groups=mesh['grp'=2,'sp'=4,'tp'=4] {'sp','tp'}, dimensions={0}, use_global_device_ids=true | all-gather | bytes 69632 | tf_op jit(solution)/shard_map/all_gather | solution.py:71
  36.2 0.8 fusion.29
  37.0 0.8 fusion.31
  37.8 20.0 %all_gather.15 = bf16[512,256]{1,0:T(8,128)(2,1)S(1)} all-gather(bf16[32,256]{1,0:T(8,128)(2,1)S(1)} %fusion.31), channel_id=1, replica_groups=mesh['grp'=2,'sp'=4,'tp'=4] {'sp','tp'}, dimensions={0}, use_global_device_ids=true | all-gather | bytes 278528 | tf_op jit(solution)/shard_map/all_gather | solution.py:70
  57.9 0.1 multiply_cosine_fusion.1
  58.0 0.0 copy-done.1
  58.1 0.3 convolution_convert_fusion
  58.4 0.0 copy-start.2
  58.4 0.3 convolution_bitcast_fusion
  58.8 0.3 fusion.42
  59.1 0.2 fusion.7
  59.2 0.6 multiply_reduce_fusion
  59.8 5.1 %all-gather = bf16[4,1,128]{2,1,0:T(2,128)(2,1)S(1)} all-gather(bf16[1,1,128]{2,1,0:T(2,128)(2,1)S(1)} %bitcast.36), channel_id=1, replica_groups=mesh['grp'=2,'sp'=4,'tp'=4] {'tp'}, dimensions={0}, use_global_device_ids=true | all-gather | bytes 1280 | tf_op jit(solution)/shard_map/all_gather | solution.py:112
  64.9 0.0 copy-done.2
  64.9 0.1 fusion.16
  65.0 7.3 %all_gather.17 = bf16[128,2048]{0,1:T(8,128)(2,1)S(1)} all-gather(bf16[128,512]{0,1:T(8,128)(2,1)S(1)} %fusion.16), channel_id=1, replica_groups=mesh['grp'=2,'sp'=4,'tp'=4] {'tp'}, dimensions={1}, use_global_device_ids=true | all-gather | bytes 655360 | tf_op jit(solution)/shard_map/all_gather | solution.py:111
  72.3 21.2 %all-gather.3.cloned.1.call-done = bf16[2048,1024]{1,0:T(8,128)(2,1)} async-done(((bf16[512,1024]{1,0:T(8,128)(2,1)}), bf16[2048,1024]{1,0:T(8,128)(2,1)}) %all-gather.3.cloned.1.call-update) | async-done | bytes 4194320 | tf_op jit(solution)/shard_map/all_gather | solution.py:119
  93.5 3.6 %fusion.3 = bf16[128,1024]{1,0:T(8,128)(2,1)} fusion(bf16[128,2048]{0,1:T(8,128)(2,1)S(1)} %all_gather.17, bf16[2048,1024]{1,0:T(8,128)(2,1)} %all-gather.3.cloned.1.call-done, f32[128]{0:T(128)S(1)} %add_rsqrt_fusion), kind=kOutput, calls=%fused_computation.8 | convolution fusion | flops 537133056 | bytes 4981248 | tf_op jit(solution)/shard_map/dot_general | solution.py:117
  (11 shorter events, 0.1 us)
Async XLA Ops:
  6.5 1.8 %copy-start = (bf16[768,768]{1,0:T(8,128)(2,1)S(1)}, bf16[768,768]{1,0:T(8,128)(2,1)}, u32[]{:S(2)}) copy-start(bf16[768,768]{1,0:T(8,128)(2,1)} %param.15) | copy-start | bytes 3538948
  6.5 51.5 %copy-start.1 = (bf16[256,512]{1,0:T(8,128)(2,1)S(1)}, bf16[256,512]{1,0:T(8,128)(2,1)}, u32[]{:S(2)}) copy-start(bf16[256,512]{1,0:T(8,128)(2,1)} %param.16) | copy-start | bytes 786436
  6.5 86.9 %all-gather.3.cloned.1.call-start = ((), (), s32[]{:S(2)}) async-start(), calls=%async_computation | async-start | bytes 5242880 | tf_op jit(solution)/shard_map/all_gather | solution.py:119
  58.4 6.5 %copy-start.2 = (f32[512]{0:T(512)S(1)}, f32[512]{0:T(512)}, u32[]{:S(2)}) copy-start(f32[512]{0:T(512)} %param.18) | copy-start | bytes 6148
Sparse Core Ops, SparseCore 0:
  8.9 84.5 all-gather.2
where the time goes:
time: 104 us
  blocking collectives  56.7 us (55%)
  waiting for transfers between devices  21.9 us (21%)
  between operations  13.5 us (13%)
  matrix products  6.45 us (6%)
  other arithmetic  4.14 us (4%)
  local copies, waits for them, and re-layouts  1.25 us (1%)
    all_gather x1, blocking collectives, on_device(): turned_keys = lax.all_gather(key_turned, ('sp', 'tp'), axis=0, tiled=True)  24.3 us
    all_gather x1, waiting for transfers between devices, on_device(): lax.all_gather(out_weight, 'sp', axis=0, tiled=True)  21.2 us
    all_gather x1, blocking collectives, on_device(): latents = lax.all_gather(latent_normed, ('sp', 'tp'), axis=0, tiled=True)  20 us
    all_gather x1, blocking collectives, on_device(): lax.all_gather(gained, 'tp', axis=1, tiled=True)  7.27 us
    all_gather x1, blocking collectives, on_device(): lax.all_gather(square_part[:, None].astype(jnp.bfloat16), 'tp', axis=1, t...  5.06 us
    dot_general x1, matrix products, on_device(): jnp.dot(all_gained, lax.all_gather(out_weight, 'sp', axis=0, tiled=True),...  3.64 us
  transfers between devices with their start and end apart: 1, of which 1 were waited for; matrix products, arithmetic and copies ran while one was open for 8% of the time, Pallas kernels for 0%

commit v1 on v0

--- a/solution.py
+++ b/solution.py
@@ -108,7 +108,7 @@
     square_part = jnp.sum(widened * widened, axis=1)
     gained = (widened * out_gain).astype(jnp.bfloat16)
     all_gained, square_parts = (
-        lax.all_gather(gained, "tp", axis=1, tiled=True),
+        jnp.concatenate(lax.all_gather(gained, "tp"), axis=1),
         lax.all_gather(square_part[:, None].astype(jnp.bfloat16), "tp", axis=1, tiled=True).astype(
             jnp.float32
         ),

time: 104 us -> 104 us (level)
  no operation moved by 1% of the time
where the time goes in v1:
time: 104 us
  blocking collectives  56.7 us (55%)
  waiting for transfers between devices  21.5 us (21%)
  between operations  13.5 us (13%)
  matrix products  6.45 us (6%)
  other arithmetic  4.04 us (4%)
  local copies, waits for them, and re-layouts  1.66 us (2%)
    all_gather x1, blocking collectives, on_device(): turned_keys = lax.all_gather(key_turned, ('sp', 'tp'), axis=0, tiled=True)  24.3 us
    all_gather x1, waiting for transfers between devices, on_device(): lax.all_gather(out_weight, 'sp', axis=0, tiled=True)  20.8 us
    all_gather x1, blocking collectives, on_device(): latents = lax.all_gather(latent_normed, ('sp', 'tp'), axis=0, tiled=True)  20 us
    all_gather x1, blocking collectives, on_device(): lax.all_gather(gained, 'tp')  7.27 us
    all_gather x1, blocking collectives, on_device(): lax.all_gather(square_part[:, None].astype(jnp.bfloat16), 'tp', axis=1, t...  5.06 us
    dot_general x1, matrix products, on_device(): jnp.dot(all_gained, lax.all_gather(out_weight, 'sp', axis=0, tiled=True),...  3.64 us
  transfers between devices with their start and end apart: 1, of which 1 were waited for; matrix products, arithmetic and copies ran while one was open for 8% of the time, Pallas kernels for 0%

profile of v1, /device:TPU:0, one launch (start us, length us, event | category | flops | bytes accessed | tf_op | source)
XLA Modules:
  0.0 103.9 jit_solution(3047194498151082465)
XLA Ops:
  6.5 0.0 copy-start
  6.5 0.0 copy-start.1
  6.5 0.0 all-gather.3.cloned.1.call-start
  6.5 0.7 all-gather.3.cloned.1.call-update
  7.3 1.0 %fusion.13 = f32[128]{0:T(128)S(1)} fusion(bf16[128,768]{1,0:T(8,128)(2,1)} %param.10), kind=kLoop, calls=%fused_computation.19 | loop fusion | flops 294784 | bytes 197120 | tf_op jit(solution)/shard_map/reduce_sum | solution.py:19
  8.3 0.0 copy-done
  8.3 1.3 %convolution_convert_fusion.1 = bf16[128,768]{1,0:T(8,128)(2,1)S(1)} fusion(bf16[768,768]{1,0:T(8,128)(2,1)S(1)} %copy-done, bf16[128,768]{1,0:T(8,128)(2,1)} %param.10, f32[768]{0:T(1024)} %param.13, f32[128]{0:T(128)S(1)} %add_rsqrt_fusion.1), kind=kOutput, calls=%fused_computation.9 | convolution fusion | flops 151486464 | bytes 1576448 | tf_op jit(solution)/shard_map/dot_general | solution.py:59
  9.6 0.2 copy.28
  9.8 0.7 convert_element_type.108
  10.5 1.1 %copy.39 = bf16[256,512]{0,1:T(8,128)(2,1)S(1)} copy(bf16[256,512]{1,0:T(8,128)(2,1)} %param.17) | data formatting | bytes 524288 | tf_op jit(solution)/shard_map/reshape | solution.py:102
  11.6 0.1 fusion.36
  11.8 0.1 pad_maximum_fusion
  11.8 24.3 %all_gather.17 = bf16[512,64]{1,0:T(8,128)(2,1)S(1)} all-gather(bf16[32,64]{1,0:T(8,128)(2,1)S(1)} %pad_maximum_fusion), channel_id=1, replica_groups=mesh['grp'=2,'sp'=4,'tp'=4] {'sp','tp'}, dimensions={0}, use_global_device_ids=true | all-gather | bytes 69632 | tf_op jit(solution)/shard_map/all_gather | solution.py:71
  36.2 0.8 fusion.28
  37.0 0.8 fusion.30
  37.8 20.0 %all_gather.16 = bf16[512,256]{1,0:T(8,128)(2,1)S(1)} all-gather(bf16[32,256]{1,0:T(8,128)(2,1)S(1)} %fusion.30), channel_id=1, replica_groups=mesh['grp'=2,'sp'=4,'tp'=4] {'sp','tp'}, dimensions={0}, use_global_device_ids=true | all-gather | bytes 278528 | tf_op jit(solution)/shard_map/all_gather | solution.py:70
  57.9 0.1 multiply_cosine_fusion.1
  58.0 0.0 copy-done.1
  58.1 0.3 convolution_convert_fusion
  58.4 0.0 copy-start.2
  58.4 0.3 convolution_bitcast_fusion
  58.8 0.3 fusion.41
  59.1 0.2 fusion.7
  59.2 0.6 multiply_reduce_fusion
  59.8 0.1 copy.34
  59.9 0.0 copy-done.2
  60.0 7.3 %all_gather.18 = bf16[4,128,512]{2,1,0:T(8,128)(2,1)S(1)} all-gather(bf16[1,128,512]{2,1,0:T(8,128)(2,1)S(1)} %multiply_convert_fusion), channel_id=1, replica_groups=mesh['grp'=2,'sp'=4,'tp'=4] {'tp'}, dimensions={0}, use_global_device_ids=true | all-gather | bytes 655360 | tf_op jit(solution)/shard_map/all_gather | solution.py:111
  67.3 0.3 copy.35
  67.5 5.1 %all-gather = bf16[4,1,128]{2,1,0:T(2,128)(2,1)S(1)} all-gather(bf16[1,1,128]{2,1,0:T(2,128)(2,1)S(1)} %bitcast.38), channel_id=1, replica_groups=mesh['grp'=2,'sp'=4,'tp'=4] {'tp'}, dimensions={0}, use_global_device_ids=true | all-gather | bytes 1280 | tf_op jit(solution)/shard_map/all_gather | solution.py:112
  72.6 20.8 %all-gather.3.cloned.1.call-done = bf16[2048,1024]{1,0:T(8,128)(2,1)} async-done(((bf16[512,1024]{1,0:T(8,128)(2,1)}), bf16[2048,1024]{1,0:T(8,128)(2,1)}) %all-gather.3.cloned.1.call-update) | async-done | bytes 4194320 | tf_op jit(solution)/shard_map/all_gather | solution.py:119
  93.5 3.6 %fusion.3 = bf16[128,1024]{1,0:T(8,128)(2,1)} fusion(bf16[128,2048]{0,1:T(8,128)(2,1)S(1)} %bitcast.32, bf16[2048,1024]{1,0:T(8,128)(2,1)} %all-gather.3.cloned.1.call-done, f32[128]{0:T(128)S(1)} %add_rsqrt_fusion), kind=kOutput, calls=%fused_computation.8 | convolution fusion | flops 537133056 | bytes 4981248 | tf_op jit(solution)/shard_map/dot_general | solution.py:117
  (12 shorter events, 0.1 us)
Async XLA Ops:
  6.5 1.8 %copy-start = (bf16[768,768]{1,0:T(8,128)(2,1)S(1)}, bf16[768,768]{1,0:T(8,128)(2,1)}, u32[]{:S(2)}) copy-start(bf16[768,768]{1,0:T(8,128)(2,1)} %param.15) | copy-start | bytes 3538948
  6.5 51.5 %copy-start.1 = (bf16[256,512]{1,0:T(8,128)(2,1)S(1)}, bf16[256,512]{1,0:T(8,128)(2,1)}, u32[]{:S(2)}) copy-start(bf16[256,512]{1,0:T(8,128)(2,1)} %param.16) | copy-start | bytes 786436
  6.5 86.9 %all-gather.3.cloned.1.call-start = ((), (), s32[]{:S(2)}) async-start(), calls=%async_computation | async-start | bytes 5242880 | tf_op jit(solution)/shard_map/all_gather | solution.py:119
  58.4 1.5 %copy-start.2 = (f32[512]{0:T(512)S(1)}, f32[512]{0:T(512)}, u32[]{:S(2)}) copy-start(f32[512]{0:T(512)} %param.18) | copy-start | bytes 6148
Sparse Core Ops, SparseCore 0:
  8.9 84.5 all-gather.2
